TPU v7x, 32 devices: a whole 2x2x4 slice. The times are simulated.
32 devices in a mesh: ep: 16 (over z, x, core), tp: 2 (over y).
Axes of the slice: x: 2, y: 2, z: 4, core: 2. Of those that a mesh axis runs over, the one named last changes fastest.
Arguments:
- hidden_in: bfloat16 [256, 2048], P('ep'), may hold values from -6 to 6
- state_in: float32 [256, 16, 64, 64], P('ep', 'tp'), may hold values from -6 to 6
- receptance: bfloat16 [256, 1024], P('ep', 'tp'), may hold values from -6 to 6
- key_in: bfloat16 [256, 1024], P('ep', 'tp'), may hold values from -1.5 to 1.5
- value_in: bfloat16 [256, 1024], P('ep', 'tp'), may hold values from -6 to 6
- learn_in: bfloat16 [256, 1024], P('ep', 'tp'), may hold values from -8 to 8
- decay_in: float32 [256, 1024], P('ep', 'tp'), may hold values from -6 to 6
- decay_base: float32 [1024], P('tp'), may hold values from -3 to 1
- norm_gain: float32 [1024], P('tp'), may hold values from 0.1 to 1.9
- out_weight: bfloat16 [1024, 2048], P('tp'), may hold values from -0.1875 to 0.1875
- routed_gain: float32 [2048], replicated, may hold values from 0.1 to 1.9
- expert_gate: bfloat16 [16, 2048, 512], P('ep', None, 'tp'), may hold values from -0.125 to 0.125
- expert_up: bfloat16 [16, 2048, 512], P('ep', None, 'tp'), may hold values from -0.125 to 0.125
- expert_down: bfloat16 [16, 512, 2048], P('ep', 'tp'), may hold values from -0.25 to 0.25
- route_ids: int32 [256, 6], P('ep'), may hold values from 0 to 15, all different within a row; in each aligned block of 16 rows (0 to 15, 16 to 31, ...) at most 12 rows name the same one
- route_weights: float32 [256, 6], P('ep'), may hold values from 0.05 to 0.5
Outputs:
- hidden_out: bfloat16 [256, 2048], P('ep')
- state_out: float32 [256, 16, 64, 64], P('ep', 'tp')
Inputs may be any that keep to these rules, and one draw needn't show every extreme that they name: `route_ids`: each row names 6 different experts. Among the rows of one index of ep no expert is named more than 12 times, a bound that some block reaches.
All inputs are finite; a program needn't handle non-finite values.
Results may differ from a plain program's by a relative error of at most 0.014.
Values may be sent and summed in bfloat16 or wider, within the bound.
A program may use at most 128 MiB of HBM per device.

v0:
```python
import functools

import jax
import jax.numpy as jnp
from jax import lax
from jax.experimental import pallas as pl
from jax.experimental.pallas import tpu as pltpu
from jax.sharding import PartitionSpec as P

EPSILON = 1e-06
GROUP_EPSILON = 0.00064
MESH = pl.DeviceIdType.MESH
F32 = jnp.float32
BF16 = jnp.bfloat16
LANES = 128


def heads_kernel(
    state_ref, read_ref, key_ref, value_ref, learn_ref, decay_ref, base_ref, gain_ref, weight_ref,
    new_ref, partial_ref, total_ref,
):
    seqs, heads, size, _ = state_ref.shape
    step = pl.program_id(0)
    reading = read_ref[...].astype(F32)
    keys = key_ref[...].astype(F32)
    values = value_ref[...].astype(F32)
    learning = jax.nn.sigmoid(learn_ref[...].astype(F32))
    decay = jnp.exp(-jax.nn.sigmoid(base_ref[...] + decay_ref[...]) * jnp.exp(F32(-0.5)))
    row = lax.broadcasted_iota(jnp.int32, (size, size), 0)
    column = lax.broadcasted_iota(jnp.int32, (size, size), 1)
    eye = (row == column).astype(F32)
    vectors = []
    for head in range(heads):
        key, read, keep, value, learn = (
            (pltpu.roll(wide, wide.shape[1] - head * size, 1) if head else wide)[:, :size]
            for wide in (keys, reading, decay, values, learning)
        )
        unit = key * lax.rsqrt(jnp.sum(key * key, axis=-1, keepdims=True) + EPSILON)
        learned = unit * learn
        learned_read = jnp.sum(learned * read, axis=-1, keepdims=True)
        key_read = jnp.sum(key * read, axis=-1, keepdims=True)
        vectors.append((unit, keep * read, value, learned, keep, key, learned_read,
                        key_read * value))

    def reduce(pair):
        head, s = pair // seqs, pair % seqs
        unit, keep_read, value = (rows[s:s + 1] for rows in vectors[head][:3])
        state = state_ref[s, head]
        return (
            jnp.sum(state * unit, axis=-1, keepdims=True),
            jnp.sum(state * keep_read, axis=-1, keepdims=True),
            jnp.sum(eye * value, axis=-1, keepdims=True),
        )

    def update(pair, carried, kept, across):
        head, s = pair // seqs, pair % seqs
        learned, keep, key, learned_read = (rows[s:s + 1] for rows in vectors[head][3:7])
        output = jnp.sum(eye * (kept - carried * learned_read), axis=0, keepdims=True)
        new_ref[s, head] = state_ref[s, head] * keep - carried * learned + across * key
        return output

    ahead = 4
    pairs = heads * seqs
    flight = [reduce(pair) for pair in range(min(ahead, pairs))]
    outputs = []
    for pair in range(pairs):
        if pair + ahead < pairs:
            flight.append(reduce(pair + ahead))
        outputs.append(update(pair, *flight[pair]))
        flight[pair] = None
    mixed = []
    for head in range(heads):
        part = slice(head * size, (head + 1) * size)
        output = jnp.concatenate(outputs[head * seqs:(head + 1) * seqs], axis=0)
        output = output + vectors[head][7]
        center = jnp.mean(output, axis=-1, keepdims=True)
        spread = jnp.mean(jnp.square(output - center), axis=-1, keepdims=True)
        mixed.append(
            (output - center) * lax.rsqrt(spread + GROUP_EPSILON) * gain_ref[:, part]
        )
    mixed = jnp.concatenate(mixed, axis=1).astype(BF16)
    product = jnp.dot(mixed, weight_ref[...], preferred_element_type=F32)

    @pl.when(step == 0)
    def _():
        total_ref[...] = product

    @pl.when(step > 0)
    def _():
        total_ref[...] += product

    @pl.when(step == pl.num_programs(0) - 1)
    def _():
        partial_ref[...] = total_ref[...].astype(BF16)


def heads_call(state_in, receptance, key_in, value_in, learn_in, decay_in, base, gain, out_weight):
    seqs, heads, size, _ = state_in.shape
    group = max(1, LANES // size)
    wide = group * size
    model = out_weight.shape[1]
    vector = pl.BlockSpec((seqs, wide), lambda i: (0, i))
    channel = pl.BlockSpec((1, wide), lambda i: (0, i))
    state = pl.BlockSpec((seqs, group, size, size), lambda i: (0, i, 0, 0))
    return pl.pallas_call(
        heads_kernel,
        grid=(heads // group,),
        in_specs=[state, vector, vector, vector, vector, vector, channel, channel,
                  pl.BlockSpec((wide, model), lambda i: (i, 0))],
        out_specs=[state, pl.BlockSpec((seqs, model), lambda i: (0, 0))],
        out_shape=[jax.ShapeDtypeStruct(state_in.shape, F32),
                   jax.ShapeDtypeStruct((seqs, model), BF16)],
        scratch_shapes=[pltpu.VMEM((seqs, model), F32)],
        compiler_params=pltpu.CompilerParams(dimension_semantics=("arbitrary",)),
    )(state_in, receptance, key_in, value_in, learn_in, decay_in, base[None], gain[None], out_weight)


def experts_kernel(
    ep, tp, inner,
    partial_ref, hidden_ref, gain_ref, ids_ref, shares_ref, gate_hbm, up_hbm, down_hbm,
    out_ref,
    gate, up, down, heads_in, residual, rows, shares, parts, from_core, summed, from_x, crossed,
    from_z, routed_in,
    load_sem, heads_send, heads_recv, share_send, share_recv, z_send, x_send, core_send, row_recv,
    core2_send, core2_recv, x2_send, x2_recv, z2_send, z2_recv, routed_send, routed_recv,
):
    width = inner // 2
    outer = ep // inner
    half = ep // 2
    me, member = lax.axis_index("ep"), lax.axis_index("tp")
    z = lax.div(me, inner)
    x = lax.div(lax.rem(me, inner), 2)
    core = lax.rem(me, 2)
    other = 1 - core

    def device(z_at, x_at, core_at):
        return z_at * inner + x_at * 2 + core_at

    def place(z_at, x_at, core_at):
        return core_at * half + z_at * width + x_at

    def send(src, dst, send_sem, recv_sem, ep_at, tp_at=None):
        copy = pltpu.make_async_remote_copy(
            src_ref=src, dst_ref=dst, send_sem=send_sem, recv_sem=recv_sem,
            device_id=(ep_at, member if tp_at is None else tp_at), device_id_type=MESH,
        )
        copy.start()
        return copy

    def arrived(ref, sem):
        pltpu.make_async_remote_copy(
            src_ref=ref, dst_ref=ref, send_sem=sem, recv_sem=sem,
            device_id=(me, member), device_id_type=MESH,
        ).wait_recv()

    barrier = pltpu.get_barrier_semaphore()
    for step in range(1, ep):
        pl.semaphore_signal(barrier, inc=1, device_id=(lax.rem(me + step, ep), member),
                            device_id_type=MESH)
    for step in range(1, tp):
        pl.semaphore_signal(barrier, inc=1, device_id=(me, lax.rem(member + step, tp)),
                            device_id_type=MESH)
    loads = [
        pltpu.make_async_copy(gate_hbm.at[0], gate, load_sem.at[0]),
        pltpu.make_async_copy(up_hbm.at[0], up, load_sem.at[1]),
        pltpu.make_async_copy(down_hbm.at[0], down, load_sem.at[2]),
    ]
    for load in loads:
        load.start()
    sent = []
    mine = place(z, x, core)
    seqs, lanes = shares.shape[1], shares.shape[2]
    lane = lax.broadcasted_iota(jnp.int32, (seqs, lanes), 1)
    down_rows = lax.broadcasted_iota(jnp.int32, (seqs, seqs), 0)
    diagonal = down_rows == lax.broadcasted_iota(jnp.int32, (seqs, seqs), 1)
    table = jnp.zeros((seqs, lanes), F32)
    for k in range(ids_ref.shape[0]):
        named = jnp.where(diagonal, ids_ref[k:k + 1, :].astype(F32), 0.0)
        share = jnp.where(diagonal, shares_ref[k:k + 1, :], 0.0)
        named = jnp.sum(named, axis=-1, keepdims=True)
        share = jnp.sum(share, axis=-1, keepdims=True)
        table += jnp.where(named == lane.astype(F32), share, 0.0)
    shares[mine] = table
    pl.semaphore_wait(barrier, ep - 1 + tp - 1)

    for step in range(1, tp):
        sent.append(send(partial_ref, heads_in.at[member], heads_send.at[step - 1],
                         heads_recv.at[member], me, lax.rem(member + step, tp)))
    heads_in[member] = partial_ref[...]
    for step in range(1, ep):
        sent.append(send(shares.at[mine], shares.at[mine], share_send.at[step - 1],
                         share_recv.at[mine], lax.rem(me + step, ep)))
    for step in range(1, tp):
        source = lax.rem(member + step, tp)
        arrived(heads_in.at[source], heads_recv.at[source])
    attention = heads_in[0].astype(F32)
    for t in range(1, tp):
        attention += heads_in[t].astype(F32)
    value = hidden_ref[...].astype(F32) + attention.astype(BF16).astype(F32)
    residual[...] = value
    scale = lax.rsqrt(jnp.mean(value * value, axis=-1, keepdims=True) + EPSILON)
    rows[mine] = (value * scale * gain_ref[...]).astype(BF16)

    def pass_x(block, base):
        for dx in range(1, width):
            sent.append(send(rows.at[block], rows.at[block], x_send.at[base * (width - 1) + dx - 1],
                             row_recv.at[block], device(z, lax.rem(x + dx, width), core)))

    def pass_core(block, base):
        sent.append(send(rows.at[block], rows.at[block], core_send.at[base], row_recv.at[block],
                         device(z, x, other)))

    for dz in range(1, outer):
        sent.append(send(rows.at[mine], rows.at[mine], z_send.at[dz - 1], row_recv.at[mine],
                         device(lax.rem(z + dz, outer), x, core)))
    pass_x(mine, 0)
    pass_core(mine, 0)
    for dz in range(1, outer):
        block = place(lax.rem(z + outer - dz, outer), x, core)
        arrived(rows.at[block], row_recv.at[block])
        pass_x(block, dz)
        pass_core(block, dz)
    count = outer
    for dz in range(outer):
        for dx in range(1, width):
            block = place(lax.rem(z + outer - dz, outer), lax.rem(x + width - dx, width), core)
            arrived(rows.at[block], row_recv.at[block])
            pass_core(block, count)
            count += 1
    for load in loads:
        load.wait()
    for step in range(1, ep):
        peer = lax.rem(me + step, ep)
        block = place(lax.div(peer, inner), lax.div(lax.rem(peer, inner), 2), lax.rem(peer, 2))
        arrived(shares.at[block], share_recv.at[block])

    take = half
    while take * seqs > 256 and take % 2 == 0:
        take //= 2
    chunk_lane = lax.broadcasted_iota(jnp.int32, (take * seqs, lanes), 1)

    def expert(first):
        block = rows[pl.ds(first, take)].reshape(take * seqs, rows.shape[2])
        gated = jnp.dot(block, gate[...], preferred_element_type=F32)
        upward = jnp.dot(block, up[...], preferred_element_type=F32)
        hidden = (jax.nn.silu(gated) * upward).astype(BF16)
        share = shares[pl.ds(first, take)].reshape(take * seqs, lanes)
        share = jnp.sum(jnp.where(chunk_lane == me, share, 0.0), axis=-1, keepdims=True)
        product = jnp.dot(hidden, down[...], preferred_element_type=F32) * share
        parts[pl.ds(first, take)] = product.astype(BF16).reshape(take, seqs, rows.shape[2])

    def experts_of(core_at):
        @pl.loop(0, half // take)
        def _(i):
            expert(core_at * half + i * take)

    experts_of(core)
    for i in range(half):
        block = other * half + i
        arrived(rows.at[block], row_recv.at[block])
    experts_of(other)

    pieces = core2_recv.shape[0]
    model = rows.shape[2]
    cuts = [pl.ds(p * (model // pieces), model // pieces) for p in range(pieces)]
    x_order = list(range(1, width)) + [0]
    z_order = list(range(1, outer)) + [0]
    for p, cut in enumerate(cuts):
        for dx in x_order:
            for dz in z_order:
                spot = lax.rem(z + dz, outer) * width + lax.rem(x + dx, width)
                sent.append(send(parts.at[other * half + spot, :, cut],
                                 from_core.at[spot, :, cut],
                                 core2_send.at[p, dx * outer + dz], core2_recv.at[p, spot],
                                 device(z, x, other)))
    for p, cut in enumerate(cuts):
        for dx in x_order:
            for dz in z_order:
                z_at = lax.rem(z + dz, outer)
                spot = z_at * width + lax.rem(x + dx, width)
                arrived(from_core.at[spot, :, cut], core2_recv.at[p, spot])
                value = (parts[core * half + spot, :, cut].astype(F32)
                         + from_core[spot, :, cut].astype(F32))
                summed[spot, :, cut] = value.astype(BF16)
                if dx:
                    sent.append(send(summed.at[spot, :, cut], from_x.at[dx - 1, z_at, :, cut],
                                     x2_send.at[p, (dx - 1) * outer + dz],
                                     x2_recv.at[p, dx - 1, z_at],
                                     device(z, lax.rem(x + dx, width), core)))
    for p, cut in enumerate(cuts):
        for dz in z_order:
            z_at = lax.rem(z + dz, outer)
            value = summed[z_at * width + x, :, cut].astype(F32)
            for dx in range(1, width):
                arrived(from_x.at[dx - 1, z_at, :, cut], x2_recv.at[p, dx - 1, z_at])
                value += from_x[dx - 1, z_at, :, cut].astype(F32)
            crossed[dz, :, cut] = value.astype(BF16)
            if dz:
                sent.append(send(crossed.at[dz, :, cut], from_z.at[dz - 1, :, cut],
                                 z2_send.at[p, dz - 1], z2_recv.at[p, dz - 1],
                                 device(z_at, x, core)))
    for p, cut in enumerate(cuts):
        value = crossed[0, :, cut].astype(F32)
        for dz in range(1, outer):
            arrived(from_z.at[dz - 1, :, cut], z2_recv.at[p, dz - 1])
            value += from_z[dz - 1, :, cut].astype(F32)
        routed_in[member, :, cut] = value.astype(BF16)
        for step in range(1, tp):
            sent.append(send(routed_in.at[member, :, cut], routed_in.at[member, :, cut],
                             routed_send.at[p, step - 1], routed_recv.at[p, member], me,
                             lax.rem(member + step, tp)))
    for p, cut in enumerate(cuts):
        for step in range(1, tp):
            source = lax.rem(member + step, tp)
            arrived(routed_in.at[source, :, cut], routed_recv.at[p, source])
        routed = routed_in[0, :, cut].astype(F32)
        for t in range(1, tp):
            routed += routed_in[t, :, cut].astype(F32)
        out_ref[:, cut] = (residual[:, cut] + routed).astype(BF16)
    for copy in sent:
        copy.wait_send()


def experts_call(inner, partial, hidden_in, gain, ids, route_weights, gate, up, down):
    ep, tp = lax.axis_size("ep"), lax.axis_size("tp")
    seqs, model = hidden_in.shape
    width, outer, half = inner // 2, ep // inner, ep // 2
    lanes = -(-ep // LANES) * LANES
    vmem = pl.BlockSpec(memory_space=pltpu.VMEM)
    hbm = pl.BlockSpec(memory_space=pltpu.HBM)
    block = (seqs, model)
    pieces = 2 if model % (2 * LANES) == 0 else 1
    dma = lambda *shape: pltpu.SemaphoreType.DMA(tuple(max(1, n) for n in shape))
    buffer = lambda *lead: pltpu.VMEM(tuple(max(1, n) for n in lead) + block, BF16)
    return pl.pallas_call(
        functools.partial(experts_kernel, ep, tp, inner),
        in_specs=[vmem] * 5 + [hbm] * 3,
        out_specs=vmem,
        out_shape=jax.ShapeDtypeStruct(block, BF16),
        scratch_shapes=[
            pltpu.VMEM(gate.shape[1:], BF16),
            pltpu.VMEM(up.shape[1:], BF16),
            pltpu.VMEM(down.shape[1:], BF16),
            buffer(tp),
            pltpu.VMEM(block, F32),
            buffer(ep),
            pltpu.VMEM((ep, seqs, lanes), F32),
            buffer(ep),
            buffer(half),
            buffer(half),
            buffer(width - 1, outer),
            buffer(outer),
            buffer(outer - 1),
            buffer(tp),
            dma(3),
            dma(tp - 1), dma(tp),
            dma(ep - 1), dma(ep),
            dma(outer - 1), dma(outer * (width - 1)), dma(half), dma(ep),
            dma(pieces, half), dma(pieces, half),
            dma(pieces, (width - 1) * outer), dma(pieces, width - 1, outer),
            dma(pieces, outer - 1), dma(pieces, outer - 1),
            dma(pieces, tp - 1), dma(pieces, tp),
        ],
        compiler_params=pltpu.CompilerParams(
            collective_id=0, has_side_effects=True, vmem_limit_bytes=60 * 1024 * 1024
        ),
    )(partial, hidden_in, gain[None], ids.T, route_weights.T, gate, up, down)


def on_device(
    inner, hidden_in, state_in, receptance, key_in, value_in, learn_in, decay_in, decay_base,
    norm_gain, out_weight, routed_gain, expert_gate, expert_up, expert_down, route_ids,
    route_weights,
):
    new_state, partial = heads_call(
        state_in, receptance, key_in, value_in, learn_in, decay_in, decay_base, norm_gain,
        out_weight,
    )
    hidden_out = experts_call(
        inner, partial, hidden_in, routed_gain, route_ids, route_weights, expert_gate, expert_up,
        expert_down,
    )
    return (hidden_out, new_state)


def plane_size(mesh):
    line = mesh.devices.reshape(mesh.shape["ep"], mesh.shape["tp"])[:, 0]
    first = getattr(line[0], "coords", None)
    if first is None:
        return min(4, len(line))
    return sum(1 for d in line if d.coords[2] == first[2])


def solution(mesh):
    in_specs = (
        P("ep", None),
        P("ep", "tp", None, None),
        P("ep", "tp"),
        P("ep", "tp"),
        P("ep", "tp"),
        P("ep", "tp"),
        P("ep", "tp"),
        P("tp"),
        P("tp"),
        P("tp", None),
        P(),
        P("ep", None, "tp"),
        P("ep", None, "tp"),
        P("ep", "tp", None),
        P("ep", None),
        P("ep", None),
    )
    out_specs = (P("ep", None), P("ep", "tp", None, None))
    return jax.shard_map(
        functools.partial(on_device, plane_size(mesh)), mesh=mesh, in_specs=in_specs,
        out_specs=out_specs, check_vma=False,
    )
```

profile of v0, /device:TPU:0, one launch (start us, length us, event | category | flops | bytes accessed | tf_op | source)
XLA Modules:
  0.0 50.1 jit_solution(3289781083476201890)
XLA Ops:
  0.6 8.3 %shard_map.167 = (f32[16,8,64,64]{3,2,1,0:T(8,128)}, bf16[16,2048]{1,0:T(8,128)(2,1)}) custom-call(f32[16,8,64,64]{3,2,1,0:T(8,128)} %state_ref.1, bf16[16,512]{1,0:T(8,128)(2,1)} %read_ref.1, bf16[16,512]{1,0:T(8,128)(2,1)} %key_ref.1, bf16[16,512]{1,0:T(8,128)(2,1)} %value_ref.1, bf16[16,512]{1,0:T(8,128)(2,1)} %learn_ref.1, f32[16,512]{1,0:T(8,128)} %decay_ref.1, ...), custom_call_target="tpu_custom_call" | custom-call | tf_op jit(solution)/shard_map/pallas_call | solution.py:105
  8.9 39.7 %shard_map.168 = bf16[16,2048]{1,0:T(8,128)(2,1)} custom-call(bf16[16,2048]{1,0:T(8,128)(2,1)} %get-tuple-element.4.partial_ref, bf16[16,2048]{1,0:T(8,128)(2,1)} %hidden_ref.1, f32[1,2048]{1,0:T(1,128)} %bitcast.5, s32[6,16]{1,0:T(8,128)} %bitcast.6, f32[6,16]{1,0:T(8,128)} %bitcast.7, bf16[1,2048,256]{2,1,0:T(8,128)(2,1)} %gate_hbm.1, ...), custom_call_target="tpu_custom_call" | custom-call | tf_op jit(solution)/shard_map/pallas_call | solution.py:335
  48.6 1.5 %copy.19 = bf16[16,2048]{1,0:T(8,128)(2,1)} copy(bf16[16,2048]{1,0:T(8,128)(2,1)} %shard_map.168) | data formatting | bytes 131072
where the time goes:
time: 50.4 us; the launch traced here: 50.1 us
  Pallas kernels  48 us (95%)
  local copies, waits for them, and re-layouts  1.47 us (3%)
  between operations  0.64 us (1%)
    pallas_call x1, Pallas kernels, experts_call(): pl.pallas_call(functools.partial(experts_kernel, ep, tp, inner), in_specs...  39.7 us
    pallas_call x1, Pallas kernels, heads_call(): pl.pallas_call(heads_kernel, grid=(heads // group,), in_specs=[state, vec...  8.27 us
    unnamed x1, local copies, waits for them, and re-layouts  1.47 us

commit v1 on v0

--- a/solution.py
+++ b/solution.py
@@ -15,113 +15,107 @@
 LANES = 128
 
 
-def heads_kernel(
-    state_ref, read_ref, key_ref, value_ref, learn_ref, decay_ref, base_ref, gain_ref, weight_ref,
-    new_ref, partial_ref, total_ref,
-):
-    seqs, heads, size, _ = state_ref.shape
-    step = pl.program_id(0)
+def split(value):
+    high = value.astype(BF16)
+    return high, (value - high.astype(F32)).astype(BF16)
+
+
+def one_head(wide, head, size):
+    first = head * size // LANES * LANES
+    tile = wide[:, first:first + max(LANES, size)]
+    offset = head * size - first
+    return (pltpu.roll(tile, tile.shape[1] - offset, 1) if offset else tile)[:, :size]
+
+
+def head_vectors(read_ref, key_ref, value_ref, learn_ref, decay_ref, base_ref, heads, size):
     reading = read_ref[...].astype(F32)
     keys = key_ref[...].astype(F32)
     values = value_ref[...].astype(F32)
     learning = jax.nn.sigmoid(learn_ref[...].astype(F32))
     decay = jnp.exp(-jax.nn.sigmoid(base_ref[...] + decay_ref[...]) * jnp.exp(F32(-0.5)))
-    row = lax.broadcasted_iota(jnp.int32, (size, size), 0)
-    column = lax.broadcasted_iota(jnp.int32, (size, size), 1)
-    eye = (row == column).astype(F32)
     vectors = []
     for head in range(heads):
         key, read, keep, value, learn = (
-            (pltpu.roll(wide, wide.shape[1] - head * size, 1) if head else wide)[:, :size]
-            for wide in (keys, reading, decay, values, learning)
+            one_head(wide, head, size) for wide in (keys, reading, decay, values, learning)
         )
         unit = key * lax.rsqrt(jnp.sum(key * key, axis=-1, keepdims=True) + EPSILON)
         learned = unit * learn
         learned_read = jnp.sum(learned * read, axis=-1, keepdims=True)
         key_read = jnp.sum(key * read, axis=-1, keepdims=True)
-        vectors.append((unit, keep * read, value, learned, keep, key, learned_read,
-                        key_read * value))
-
-    def reduce(pair):
-        head, s = pair // seqs, pair % seqs
-        unit, keep_read, value = (rows[s:s + 1] for rows in vectors[head][:3])
-        state = state_ref[s, head]
-        return (
-            jnp.sum(state * unit, axis=-1, keepdims=True),
-            jnp.sum(state * keep_read, axis=-1, keepdims=True),
-            jnp.sum(eye * value, axis=-1, keepdims=True),
-        )
-
-    def update(pair, carried, kept, across):
-        head, s = pair // seqs, pair % seqs
-        learned, keep, key, learned_read = (rows[s:s + 1] for rows in vectors[head][3:7])
-        output = jnp.sum(eye * (kept - carried * learned_read), axis=0, keepdims=True)
-        new_ref[s, head] = state_ref[s, head] * keep - carried * learned + across * key
-        return output
-
-    ahead = 4
-    pairs = heads * seqs
-    flight = [reduce(pair) for pair in range(min(ahead, pairs))]
-    outputs = []
-    for pair in range(pairs):
-        if pair + ahead < pairs:
-            flight.append(reduce(pair + ahead))
-        outputs.append(update(pair, *flight[pair]))
-        flight[pair] = None
+        unit_high, unit_low = split(unit)
+        read_high, read_low = split(keep * read)
+        probe = jnp.concatenate([unit_high, read_high, unit_low, read_low], axis=0)
+        vectors.append((probe, value, learned, keep, key, learned_read, key_read * value))
+    return vectors
+
+
+def own_lanes(seqs, size):
+    row = lax.broadcasted_iota(jnp.int32, (seqs, seqs * size), 0)
+    lane = lax.broadcasted_iota(jnp.int32, (seqs, seqs * size), 1)
+    return row == lane // size
+
+
+def folded(wide, size):
+    step = max(LANES, size)
+    total = wide[:, :step]
+    for first in range(step, wide.shape[1], step):
+        total += wide[:, first:first + step]
+    for part in range(1, step // size):
+        total += pltpu.roll(total, step // 2, 1) if part == step // size // 2 else 0.0
+    return total[:, :size]
+
+
+def read_head(state, vectors, own):
+    seqs, size = vectors[1].shape
+    probe = vectors[0]
+    high, low = split(state.reshape(seqs * size, size))
+    along = (((1,), (1,)), ((), ()))
+    first = lax.dot_general(probe, high, along, preferred_element_type=F32)
+    second = lax.dot_general(probe[:2 * seqs], low, along, preferred_element_type=F32)
+    both = first[:2 * seqs] + first[2 * seqs:] + second
+    carried = jnp.where(own, both[:seqs], 0.0)
+    kept = jnp.where(own, both[seqs:], 0.0)
+    output = folded(kept, size) - folded(carried, size) * vectors[5] + vectors[6]
+    return carried, output
+
+
+def update_head(state, carried, vectors, own):
+    _, value, learned, keep, key = vectors[:5]
+    seqs, size = value.shape
+    carried_high, carried_low = split(carried)
+    learned_high, learned_low = split(learned)
+    twice = jnp.concatenate([value] * max(1, LANES // size), axis=1)
+    spread = jnp.concatenate([twice] * (seqs * size // twice.shape[1]), axis=1)
+    spread = jnp.where(own, spread, 0.0).astype(BF16)
+    left = jnp.concatenate([carried_high, carried_low, carried_high, spread], axis=0)
+    right = jnp.concatenate(
+        [-learned_high, -learned_high, -learned_low, key.astype(BF16)], axis=0)
+    change = lax.dot_general(left, right, (((0,), (0,)), ((), ())), preferred_element_type=F32)
+    return state * keep[:, None, :] + change.reshape(seqs, size, size)
+
+
+def mix(outputs, gain_ref):
+    size = outputs[0].shape[1]
     mixed = []
-    for head in range(heads):
-        part = slice(head * size, (head + 1) * size)
-        output = jnp.concatenate(outputs[head * seqs:(head + 1) * seqs], axis=0)
-        output = output + vectors[head][7]
+    for head, output in enumerate(outputs):
         center = jnp.mean(output, axis=-1, keepdims=True)
         spread = jnp.mean(jnp.square(output - center), axis=-1, keepdims=True)
-        mixed.append(
-            (output - center) * lax.rsqrt(spread + GROUP_EPSILON) * gain_ref[:, part]
-        )
-    mixed = jnp.concatenate(mixed, axis=1).astype(BF16)
-    product = jnp.dot(mixed, weight_ref[...], preferred_element_type=F32)
-
-    @pl.when(step == 0)
-    def _():
-        total_ref[...] = product
-
-    @pl.when(step > 0)
-    def _():
-        total_ref[...] += product
-
-    @pl.when(step == pl.num_programs(0) - 1)
-    def _():
-        partial_ref[...] = total_ref[...].astype(BF16)
-
-
-def heads_call(state_in, receptance, key_in, value_in, learn_in, decay_in, base, gain, out_weight):
-    seqs, heads, size, _ = state_in.shape
-    group = max(1, LANES // size)
-    wide = group * size
-    model = out_weight.shape[1]
-    vector = pl.BlockSpec((seqs, wide), lambda i: (0, i))
-    channel = pl.BlockSpec((1, wide), lambda i: (0, i))
-    state = pl.BlockSpec((seqs, group, size, size), lambda i: (0, i, 0, 0))
-    return pl.pallas_call(
-        heads_kernel,
-        grid=(heads // group,),
-        in_specs=[state, vector, vector, vector, vector, vector, channel, channel,
-                  pl.BlockSpec((wide, model), lambda i: (i, 0))],
-        out_specs=[state, pl.BlockSpec((seqs, model), lambda i: (0, 0))],
-        out_shape=[jax.ShapeDtypeStruct(state_in.shape, F32),
-                   jax.ShapeDtypeStruct((seqs, model), BF16)],
-        scratch_shapes=[pltpu.VMEM((seqs, model), F32)],
-        compiler_params=pltpu.CompilerParams(dimension_semantics=("arbitrary",)),
-    )(state_in, receptance, key_in, value_in, learn_in, decay_in, base[None], gain[None], out_weight)
-
-
-def experts_kernel(
+        gain = one_head(gain_ref[...], head, size)
+        mixed.append((output - center) * lax.rsqrt(spread + GROUP_EPSILON) * gain)
+    return jnp.concatenate(mixed, axis=1).astype(BF16)
+
+
+def layer_kernel(
     ep, tp, inner,
-    partial_ref, hidden_ref, gain_ref, ids_ref, shares_ref, gate_hbm, up_hbm, down_hbm,
-    out_ref,
+    state_hbm, read_hbm, key_hbm, value_hbm, learn_hbm, decay_hbm, base_hbm, norm_hbm, weight_hbm,
+    hidden_hbm, gain_hbm, ids_hbm, shares_hbm, gate_hbm, up_hbm, down_hbm,
+    out_ref, new_ref,
+    state_ref, read_ref, key_ref, value_ref, learn_ref, decay_ref, base_ref, norm_ref, weight_ref,
+    hidden_ref, gain_ref, ids_ref, shares_ref, carried_ref,
     gate, up, down, heads_in, residual, rows, shares, parts, from_core, summed, from_x, crossed,
     from_z, routed_in,
-    load_sem, heads_send, heads_recv, share_send, share_recv, z_send, x_send, core_send, row_recv,
+    vector_sem, state_sem, weight_sem, load_sem,
+    heads_send, heads_recv, share_send, share_recv, z_send, x_send, core_send, row_recv,
     core2_send, core2_recv, x2_send, x2_recv, z2_send, z2_recv, routed_send, routed_recv,
 ):
     width = inner // 2
@@ -153,6 +147,25 @@
             device_id=(me, member), device_id_type=MESH,
         ).wait_recv()
 
+    vector_pairs = [
+        (read_hbm, read_ref), (key_hbm, key_ref), (value_hbm, value_ref), (learn_hbm, learn_ref),
+        (decay_hbm, decay_ref), (base_hbm, base_ref), (norm_hbm, norm_ref),
+        (hidden_hbm, hidden_ref), (gain_hbm, gain_ref), (ids_hbm, ids_ref),
+        (shares_hbm, shares_ref),
+    ]
+    vector_loads = [pltpu.make_async_copy(source, target, vector_sem.at[i])
+                    for i, (source, target) in enumerate(vector_pairs)]
+    seqs, heads, size, _ = state_hbm.shape
+    state_loads = [pltpu.make_async_copy(state_hbm.at[:, head], state_ref.at[head],
+                                         state_sem.at[head]) for head in range(heads)]
+    weight_load = pltpu.make_async_copy(weight_hbm, weight_ref, weight_sem.at[0])
+    loads = [
+        pltpu.make_async_copy(gate_hbm.at[0], gate, load_sem.at[0]),
+        pltpu.make_async_copy(up_hbm.at[0], up, load_sem.at[1]),
+        pltpu.make_async_copy(down_hbm.at[0], down, load_sem.at[2]),
+    ]
+    for load in vector_loads + state_loads + [weight_load] + loads:
+        load.start()
     barrier = pltpu.get_barrier_semaphore()
     for step in range(1, ep):
         pl.semaphore_signal(barrier, inc=1, device_id=(lax.rem(me + step, ep), member),
@@ -160,16 +173,33 @@
     for step in range(1, tp):
         pl.semaphore_signal(barrier, inc=1, device_id=(me, lax.rem(member + step, tp)),
                             device_id_type=MESH)
-    loads = [
-        pltpu.make_async_copy(gate_hbm.at[0], gate, load_sem.at[0]),
-        pltpu.make_async_copy(up_hbm.at[0], up, load_sem.at[1]),
-        pltpu.make_async_copy(down_hbm.at[0], down, load_sem.at[2]),
-    ]
-    for load in loads:
-        load.start()
+    for load in vector_loads:
+        load.wait()
+    vectors = head_vectors(read_ref, key_ref, value_ref, learn_ref, decay_ref, base_ref, heads,
+                           size)
+    own = own_lanes(seqs, size)
+    outputs = []
+    for head in range(heads):
+        state_loads[head].wait()
+        carried, output = read_head(state_ref[head], vectors[head], own)
+        carried_ref[head] = carried
+        outputs.append(output)
+    mixed = mix(outputs, norm_ref)
+    weight_load.wait()
+    pl.semaphore_wait(barrier, ep - 1 + tp - 1)
     sent = []
+    model = rows.shape[2]
+    slices = heads_send.shape[0]
+    spans = [pl.ds(p * (model // slices), model // slices) for p in range(slices)]
+    for p, span in enumerate(spans):
+        product = jnp.dot(mixed, weight_ref[:, span], preferred_element_type=F32)
+        heads_in[member, :, span] = product.astype(BF16)
+        for step in range(1, tp):
+            sent.append(send(heads_in.at[member, :, span], heads_in.at[member, :, span],
+                             heads_send.at[p, step - 1], heads_recv.at[p, member], me,
+                             lax.rem(member + step, tp)))
     mine = place(z, x, core)
-    seqs, lanes = shares.shape[1], shares.shape[2]
+    lanes = shares.shape[2]
     lane = lax.broadcasted_iota(jnp.int32, (seqs, lanes), 1)
     down_rows = lax.broadcasted_iota(jnp.int32, (seqs, seqs), 0)
     diagonal = down_rows == lax.broadcasted_iota(jnp.int32, (seqs, seqs), 1)
@@ -181,18 +211,15 @@
         share = jnp.sum(share, axis=-1, keepdims=True)
         table += jnp.where(named == lane.astype(F32), share, 0.0)
     shares[mine] = table
-    pl.semaphore_wait(barrier, ep - 1 + tp - 1)
-
-    for step in range(1, tp):
-        sent.append(send(partial_ref, heads_in.at[member], heads_send.at[step - 1],
-                         heads_recv.at[member], me, lax.rem(member + step, tp)))
-    heads_in[member] = partial_ref[...]
     for step in range(1, ep):
         sent.append(send(shares.at[mine], shares.at[mine], share_send.at[step - 1],
                          share_recv.at[mine], lax.rem(me + step, ep)))
-    for step in range(1, tp):
-        source = lax.rem(member + step, tp)
-        arrived(heads_in.at[source], heads_recv.at[source])
+    for head in range(heads):
+        new_ref[:, head] = update_head(state_ref[head], carried_ref[head], vectors[head], own)
+    for p, span in enumerate(spans):
+        for step in range(1, tp):
+            source = lax.rem(member + step, tp)
+            arrived(heads_in.at[source, :, span], heads_recv.at[p, source])
     attention = heads_in[0].astype(F32)
     for t in range(1, tp):
         attention += heads_in[t].astype(F32)
@@ -261,7 +288,6 @@
     experts_of(other)
 
     pieces = core2_recv.shape[0]
-    model = rows.shape[2]
     cuts = [pl.ds(p * (model // pieces), model // pieces) for p in range(pieces)]
     x_order = list(range(1, width)) + [0]
     z_order = list(range(1, outer)) + [0]
@@ -321,23 +347,31 @@
         copy.wait_send()
 
 
-def experts_call(inner, partial, hidden_in, gain, ids, route_weights, gate, up, down):
+def layer_call(
+    inner, state_in, receptance, key_in, value_in, learn_in, decay_in, base, norm, out_weight,
+    hidden_in, gain, ids, route_weights, gate, up, down,
+):
     ep, tp = lax.axis_size("ep"), lax.axis_size("tp")
     seqs, model = hidden_in.shape
+    heads, size = state_in.shape[1:3]
     width, outer, half = inner // 2, ep // inner, ep // 2
     lanes = -(-ep // LANES) * LANES
-    vmem = pl.BlockSpec(memory_space=pltpu.VMEM)
     hbm = pl.BlockSpec(memory_space=pltpu.HBM)
     block = (seqs, model)
     pieces = 2 if model % (2 * LANES) == 0 else 1
+    slices = 4 if model % (4 * LANES) == 0 else 1
     dma = lambda *shape: pltpu.SemaphoreType.DMA(tuple(max(1, n) for n in shape))
     buffer = lambda *lead: pltpu.VMEM(tuple(max(1, n) for n in lead) + block, BF16)
+    small = [receptance, key_in, value_in, learn_in, decay_in, base[None], norm[None], out_weight,
+             hidden_in, gain[None], ids.T, route_weights.T]
     return pl.pallas_call(
-        functools.partial(experts_kernel, ep, tp, inner),
-        in_specs=[vmem] * 5 + [hbm] * 3,
-        out_specs=vmem,
-        out_shape=jax.ShapeDtypeStruct(block, BF16),
+        functools.partial(layer_kernel, ep, tp, inner),
+        in_specs=[hbm] * 16,
+        out_shape=[pltpu.VMEM(block, BF16), pltpu.VMEM(state_in.shape, F32)],
         scratch_shapes=[
+            pltpu.VMEM((heads, seqs, size, size), F32),
+            *[pltpu.VMEM(array.shape, array.dtype) for array in small],
+            pltpu.VMEM((heads, seqs, seqs * size), F32),
             pltpu.VMEM(gate.shape[1:], BF16),
             pltpu.VMEM(up.shape[1:], BF16),
             pltpu.VMEM(down.shape[1:], BF16),
@@ -352,8 +386,8 @@
             buffer(outer),
             buffer(outer - 1),
             buffer(tp),
-            dma(3),
-            dma(tp - 1), dma(tp),
+            dma(len(small) - 1), dma(heads), dma(1), dma(3),
+            dma(slices, tp - 1), dma(slices, tp),
             dma(ep - 1), dma(ep),
             dma(outer - 1), dma(outer * (width - 1)), dma(half), dma(ep),
             dma(pieces, half), dma(pieces, half),
@@ -362,9 +396,9 @@
             dma(pieces, tp - 1), dma(pieces, tp),
         ],
         compiler_params=pltpu.CompilerParams(
-            collective_id=0, has_side_effects=True, vmem_limit_bytes=60 * 1024 * 1024
+            collective_id=0, has_side_effects=True, vmem_limit_bytes=58 * 1024 * 1024
         ),
-    )(partial, hidden_in, gain[None], ids.T, route_weights.T, gate, up, down)
+    )(state_in, *small, gate, up, down)
 
 
 def on_device(
@@ -372,12 +406,9 @@
     norm_gain, out_weight, routed_gain, expert_gate, expert_up, expert_down, route_ids,
     route_weights,
 ):
-    new_state, partial = heads_call(
-        state_in, receptance, key_in, value_in, learn_in, decay_in, decay_base, norm_gain,
-        out_weight,
-    )
-    hidden_out = experts_call(
-        inner, partial, hidden_in, routed_gain, route_ids, route_weights, expert_gate, expert_up,
+    hidden_out, new_state = layer_call(
+        inner, state_in, receptance, key_in, value_in, learn_in, decay_in, decay_base, norm_gain,
+        out_weight, hidden_in, routed_gain, route_ids, route_weights, expert_gate, expert_up,
         expert_down,
     )
     return (hidden_out, new_state)

time: 50.4 us -> 45.2 us (0.90)
  Pallas kernels: 48 us -> 41.7 us
  local copies, waits for them, and re-layouts: 1.47 us -> 2.64 us
    pallas_call x2 -> x1, Pallas kernels: 48 us -> 41.7 us  [layer_call(): pl.pallas_call(functools.partial(layer_kernel, ep, tp, inner), in_specs=[...]
    unnamed x1 -> x2, local copies, waits for them, and re-layouts: 1.47 us -> 2.64 us
where the time goes in v1:
time: 45.2 us; the launch traced here: 45 us
  Pallas kernels  41.7 us (92%)
  local copies, waits for them, and re-layouts  2.64 us (6%)
  between operations  0.65 us (1%)
    pallas_call x1, Pallas kernels, layer_call(): pl.pallas_call(functools.partial(layer_kernel, ep, tp, inner), in_specs=[...  41.7 us
    unnamed x2, local copies, waits for them, and re-layouts  2.64 us

profile of v1, /device:TPU:0, one launch (start us, length us, event | category | flops | bytes accessed | tf_op | source)
XLA Modules:
  0.0 45.0 jit_solution(6837699246184940241)
XLA Ops:
  0.6 41.7 %shard_map.167 = (bf16[16,2048]{1,0:T(8,128)(2,1)S(1)}, f32[16,8,64,64]{3,2,1,0:T(8,128)S(1)}) custom-call(f32[16,8,64,64]{3,2,1,0:T(8,128)} %state_hbm.1, bf16[16,512]{1,0:T(8,128)(2,1)} %read_hbm.1, bf16[16,512]{1,0:T(8,128)(2,1)} %key_hbm.1, bf16[16,512]{1,0:T(8,128)(2,1)} %value_hbm.1, bf16[16,512]{1,0:T(8,128)(2,1)} %learn_hbm.1, f32[16,512]{1,0:T(8,128)} %decay_hbm.1, ...), custom_call_target="tpu_custom_call" | custom-call | tf_op jit(solution)/shard_map/pallas_call | solution.py:367
  42.3 0.6 %copy.20 = bf16[16,2048]{1,0:T(8,128)(2,1)} copy(bf16[16,2048]{1,0:T(8,128)(2,1)S(1)} %get-tuple-element.2) | data formatting | bytes 131072
  43.0 2.0 %copy.21 = f32[16,8,64,64]{3,2,1,0:T(8,128)} copy(f32[16,8,64,64]{3,2,1,0:T(8,128)S(1)} %get-tuple-element.3) | data formatting | bytes 4194304
